TPU v7x, 32 devices: a whole 2x2x4 slice. The times are simulated.
32 devices in a mesh: ep: 16 (over z, y, x), tp: 2 (over core).
Axes of the slice: x: 2, y: 2, z: 4, core: 2. Of those that a mesh axis runs over, the one named last changes fastest.
Arguments:
- inputs: bfloat16 [1024, 2048], P('ep'), may hold values from -6 to 6
- cache_keys: bfloat16 [1024, 2, 64, 1024], P('ep', 'tp'), may hold values from -6 to 6
- cache_values: bfloat16 [1024, 2, 64, 1024], P('ep', 'tp'), may hold values from -12 to 12
- lengths: int32 [1024], P('ep'), may hold values from 1 to 1024, as said below
- query_weight: bfloat16 [2048, 1024], P(None, 'tp'), may hold values from -0.125 to 0.125
- key_weight: bfloat16 [2048, 128], P(None, 'tp'), may hold values from -0.125 to 0.125
- value_weight: bfloat16 [2048, 128], P(None, 'tp'), may hold values from -0.125 to 0.125
- head_bias: float32 [16], P('tp'), may hold values from -7 to -3
- out_weight: bfloat16 [1024, 2048], P('tp'), may hold values from -0.75 to 0.75
- attend_gain: float32 [2048], replicated, may hold values from 0.1 to 1.9
- router_weight: bfloat16 [2048, 16], replicated, may hold values from -0.125 to 0.125
- routes: int32 [1024, 4], P('ep'), may hold values from 0 to 15, all different within a row; in each aligned block of 64 rows (0 to 63, 64 to 127, ...) at most 32 rows name the same one
- expert_gate: bfloat16 [16, 2048, 512], P('ep', None, 'tp'), may hold values from -0.125 to 0.125
- expert_up: bfloat16 [16, 2048, 512], P('ep', None, 'tp'), may hold values from -0.125 to 0.125
- expert_down: bfloat16 [16, 512, 2048], P('ep', 'tp'), may hold values from -0.25 to 0.25
- shared_gate: bfloat16 [2048, 512], P(None, 'tp'), may hold values from -0.125 to 0.125
- shared_up: bfloat16 [2048, 512], P(None, 'tp'), may hold values from -0.125 to 0.125
- shared_down: bfloat16 [512, 2048], P('tp'), may hold values from -0.25 to 0.25
- final_gain: float32 [2048], P('tp'), may hold values from 0.1 to 1.9
Outputs:
- output: bfloat16 [1024, 2048], P('ep', 'tp')
- new_keys: bfloat16 [1024, 128], P('ep', 'tp')
- new_values: bfloat16 [1024, 128], P('ep', 'tp')
Inputs may be any that keep to these rules, and one draw needn't show every extreme that they name: `lengths`: some sequence has 1024 filled positions and some other has 1. `routes`: each row names 4 different experts. Among the 64 rows of one index of ep no expert is named more than 32 times; some expert is named exactly 32 times by the rows of some index.
All inputs are finite; a program needn't handle non-finite values.
Results may differ from a plain program's by a relative error of at most 0.015.
Values may be sent and summed in bfloat16 or wider, within the bound.
A program may use at most 128 MiB of HBM per device.

v0:
```python
import math
import jax
import jax.numpy as jnp
from jax import lax
from jax.sharding import PartitionSpec as P

RESIDUAL_SCALE = 2.0**0.25
ROUTE_SCALE = 2.5
NORM_EPS = 1e-05


def layer_norm(values, gain_vec):
    row_mean = jnp.mean(values, axis=-1, keepdims=True)
    centered = values - row_mean
    row_var = jnp.mean(centered * centered, axis=-1, keepdims=True)
    return centered * lax.rsqrt(row_var + NORM_EPS) * gain_vec


def strictly_later(size):
    row_pos = lax.broadcasted_iota(jnp.int32, (size, size), 0)
    col_pos = lax.broadcasted_iota(jnp.int32, (size, size), 1)
    return (row_pos > col_pos).astype(jnp.float32)


def later_totals(log_keep):
    lead = log_keep.shape[:-1]
    length = log_keep.shape[-1]
    block_size = math.gcd(length, 128)
    block_count = length // block_size
    blocked = log_keep.reshape(lead + (block_count, block_size))
    inside = jnp.einsum(
        "...bi,ic->...bc", blocked, strictly_later(block_size), precision=lax.Precision.HIGHEST
    )
    block_total = jnp.sum(blocked, axis=-1)
    after = jnp.einsum(
        "...i,ic->...c", block_total, strictly_later(block_count), precision=lax.Precision.HIGHEST
    )
    return (inside + after[..., None]).reshape(lead + (length,))


def on_device(
    inputs,
    cache_keys,
    cache_values,
    lengths,
    query_weight,
    key_weight,
    value_weight,
    head_bias,
    out_weight,
    attend_gain,
    router_weight,
    routes,
    expert_gate,
    expert_up,
    expert_down,
    shared_gate,
    shared_up,
    shared_down,
    final_gain,
):
    seq_count, model_width = inputs.shape
    key_heads, head_size, cache_length = cache_keys.shape[1:]
    query_heads = head_bias.shape[0]
    groups = query_heads // key_heads
    choices_count = routes.shape[1]
    experts = router_weight.shape[1]
    core_index = lax.axis_index("tp")
    half_width = model_width // lax.axis_size("tp")
    query = jnp.dot(inputs, query_weight, preferred_element_type=jnp.float32).astype(jnp.bfloat16)
    query = query.reshape(seq_count, key_heads, groups, head_size)
    new_keys = jnp.dot(inputs, key_weight, preferred_element_type=jnp.float32).astype(jnp.bfloat16)
    new_values = jnp.dot(inputs, value_weight, preferred_element_type=jnp.float32).astype(
        jnp.bfloat16
    )
    scores = jnp.einsum("skgd,skdc->skgc", query, cache_keys, preferred_element_type=jnp.float32)
    scores = scores * head_size ** (-0.5) + head_bias.reshape(key_heads, groups)[None, :, :, None]
    usable = (
        lax.broadcasted_iota(jnp.int32, (1, 1, 1, cache_length), 3) < lengths[:, None, None, None]
    )
    log_keep = jnp.where(usable, jax.nn.log_sigmoid(-scores), 0.0)
    later_sum = later_totals(log_keep)
    stick_weight = jnp.where(usable, jnp.exp(jax.nn.log_sigmoid(scores) + later_sum), 0.0).astype(
        jnp.bfloat16
    )
    attended = jnp.einsum(
        "skgc,skdc->skgd", stick_weight, cache_values, preferred_element_type=jnp.float32
    )
    attended = attended.astype(jnp.bfloat16).reshape(seq_count, query_heads * head_size)
    attention = lax.psum(
        jnp.dot(attended, out_weight, preferred_element_type=jnp.float32).astype(jnp.bfloat16), "tp"
    ).astype(jnp.float32)
    hidden = layer_norm(
        RESIDUAL_SCALE * inputs.astype(jnp.float32) + attention, attend_gain
    ).astype(jnp.bfloat16)
    router_probs = jax.nn.sigmoid(
        jnp.dot(hidden, router_weight, preferred_element_type=jnp.float32)
    )
    picked = routes[:, :, None] == lax.broadcasted_iota(jnp.int32, (1, 1, experts), 2)
    chosen = jnp.sum(jnp.where(picked, router_probs[:, None, :], 0.0), axis=2)
    route_weights = ROUTE_SCALE * chosen / jnp.sum(chosen, axis=1, keepdims=True)
    capacity = 2 * seq_count * choices_count // experts
    row_total = seq_count * choices_count
    onehot_float = picked.reshape(row_total, experts).astype(jnp.float32)
    earlier_count = jnp.dot(
        strictly_later(row_total), onehot_float, precision=lax.Precision.HIGHEST
    )
    slot_index = jnp.sum(earlier_count * onehot_float, axis=1).astype(jnp.int32)
    target = routes.reshape(-1) * capacity + slot_index
    selector_float = (
        target[:, None] == lax.broadcasted_iota(jnp.int32, (1, experts * capacity), 1)
    ).astype(jnp.float32)
    selector = selector_float.astype(jnp.bfloat16)
    placement = jnp.sum(selector_float.reshape(seq_count, choices_count, -1), axis=1).astype(
        jnp.bfloat16
    )
    outgoing = lax.dot_general(
        placement, hidden, (((0,), (0,)), ((), ())), preferred_element_type=jnp.float32
    )
    outgoing = outgoing.astype(jnp.bfloat16).reshape(experts, capacity, -1)
    arrived = lax.all_to_all(outgoing, "ep", split_axis=0, concat_axis=0, tiled=True)
    senders, slot_count, _ = arrived.shape
    flat_rows = arrived.reshape(senders * slot_count, -1)
    gate_act = jnp.dot(flat_rows, expert_gate[0], preferred_element_type=jnp.float32)
    up_act = jnp.dot(flat_rows, expert_up[0], preferred_element_type=jnp.float32)
    inner = (jax.nn.silu(gate_act) * up_act).astype(jnp.bfloat16)
    partial_value = jnp.dot(inner, expert_down[0], preferred_element_type=jnp.float32)
    summed = lax.psum_scatter(
        partial_value.astype(jnp.bfloat16), "tp", scatter_dimension=1, tiled=True
    )
    back_rows = summed.reshape(senders, slot_count, -1)
    returned = lax.all_to_all(back_rows, "ep", split_axis=0, concat_axis=0, tiled=True)
    gathered = jnp.dot(
        selector, returned.reshape(experts * capacity, -1), preferred_element_type=jnp.float32
    )
    gathered = gathered.reshape(seq_count, choices_count, -1)
    routed = jnp.sum(route_weights[:, :, None] * gathered, axis=1)
    shared_g = jnp.dot(hidden, shared_gate, preferred_element_type=jnp.float32)
    shared_u = jnp.dot(hidden, shared_up, preferred_element_type=jnp.float32)
    shared_inner = (jax.nn.silu(shared_g) * shared_u).astype(jnp.bfloat16)
    shared_partial = jnp.dot(shared_inner, shared_down, preferred_element_type=jnp.float32)
    shared_result = lax.psum_scatter(
        shared_partial.astype(jnp.bfloat16), "tp", scatter_dimension=1, tiled=True
    ).astype(jnp.float32)
    own_hidden = lax.dynamic_slice_in_dim(hidden, core_index * half_width, half_width, 1)
    mixed_rows = RESIDUAL_SCALE * own_hidden.astype(jnp.float32) + routed + shared_result
    totals = lax.psum((jnp.sum(mixed_rows, axis=1), jnp.sum(mixed_rows * mixed_rows, axis=1)), "tp")
    row_mean = totals[0] / model_width
    row_var = totals[1] / model_width - row_mean * row_mean
    normed = (mixed_rows - row_mean[:, None]) * lax.rsqrt(row_var + NORM_EPS)[:, None]
    output = (normed * final_gain).astype(jnp.bfloat16)
    return (output, new_keys, new_values)


def solution(mesh):
    placed = (
        P("ep", None),
        P("ep", "tp", None, None),
        P("ep", "tp", None, None),
        P("ep"),
        P(None, "tp"),
        P(None, "tp"),
        P(None, "tp"),
        P("tp"),
        P("tp", None),
        P(),
        P(),
        P("ep", None),
        P("ep", None, "tp"),
        P("ep", None, "tp"),
        P("ep", "tp", None),
        P(None, "tp"),
        P(None, "tp"),
        P("tp", None),
        P("tp"),
    )
    return jax.shard_map(
        on_device,
        mesh=mesh,
        in_specs=placed,
        out_specs=(P("ep", "tp"), P("ep", "tp"), P("ep", "tp")),
        check_vma=False,
    )
```

profile of v0, /device:TPU:9, one launch (start us, length us, event | category | flops | bytes accessed | tf_op | source)
XLA Modules:
  0.0 174.9 jit_solution(5036537996058150898)
XLA Ops:
  7.2 0.0 copy-start
  7.2 0.0 copy-start.10
  7.2 0.0 all-reduce.3.cloned.1.call-start
  7.2 2.3 %convolution_convert_fusion.4 = bf16[64,512]{1,0:T(8,128)(2,1)S(1)} fusion(bf16[64,2048]{1,0:T(8,128)(2,1)} %param.19, bf16[2048,512]{1,0:T(8,128)(2,1)} %param.23), kind=kOutput, calls=%fused_computation.27 | convolution fusion | flops 134250496 | bytes 2424832 | tf_op jit(solution)/shard_map/dot_general | solution.py:70
  9.5 0.1 reshape.201
  9.7 0.0 copy-done.10
  9.7 0.1 iota_compare_fusion.3
  9.8 0.0 copy-start.11
  9.8 4.6 %fusion.2 = f32[64,8,1024]{2,1,0:T(8,128)S(1)} fusion(bf16[64,8,64]{2,1,0:T(8,128)(2,1)S(1)} %reshape.201, bf16[64,1,64,1024]{3,2,1,0:T(8,128)(2,1)} %param.20), kind=kOutput, calls=%fused_computation.2 | convolution fusion | flops 67108864 | bytes 10551296 | tf_op jit(solution)/shard_map/skgd,skdc->skgc/dot_general | solution.py:76
  14.4 0.0 copy-done.11
  14.4 3.0 %fusion.65 = (f32[64,8,8]{1,2,0:T(8,128)S(1)}, f32[64,8,8,128]{3,1,2,0:T(8,128)}) fusion(f32[8]{0:T(128)S(1)} %copy-done.11, f32[64,8,1024]{2,1,0:T(8,128)S(1)} %fusion.2, pred[64,1024]{1,0:T(8,128)(4,1)S(1)} %iota_compare_fusion.3), kind=kLoop, calls=%fused_computation.95 | loop fusion | flops 5763072 | bytes 4276256 | tf_op jit(solution)/shard_map/reduce_sum | solution.py:34
  17.4 0.0 copy-done.1
  17.4 0.1 copy.53
  17.5 0.2 fusion.58
  17.7 0.1 copy.54
  17.8 4.2 %fusion.14 = f32[64,8,8,128]{3,2,1,0:T(8,128)} fusion(f32[64,8,8,128]{3,1,2,0:T(8,128)} %get-tuple-element.11, f32[64,8,8]{2,1,0:T(8,128)S(1)} %copy.54), kind=kOutput, calls=%fused_computation.21 | convolution fusion | flops 805847040 | bytes 4210688 | tf_op jit(solution)/shard_map/...bi,ic->...bc/dot_general | solution.py:31
  22.0 2.7 %reshape.204 = f32[64,8,1024]{2,1,0:T(8,128)} reshape(f32[64,8,8,128]{3,2,1,0:T(8,128)} %fusion.14) | data formatting | bytes 4194304 | tf_op jit(solution)/shard_map/reshape | solution.py:38
  24.7 7.0 %fusion.19 = bf16[64,8,64]{2,1,0:T(8,128)(2,1)S(1)} fusion(bf16[64,1,64,1024]{3,2,1,0:T(8,128)(2,1)} %param.21, f32[64,8,1024]{2,1,0:T(8,128)} %reshape.204, f32[64,8,1024]{2,1,0:T(8,128)} %copy-done.1, f32[8]{0:T(128)S(1)} %copy-done.11, pred[64,1024]{1,0:T(8,128)(4,1)S(1)} %iota_compare_fusion.3), kind=kOutput, calls=%fused_computation.26 | convolution fusion | flops 73957376 | bytes 12714016 | tf_op jit(solution)/shard_map/skgc,skdc->skgd/dot_general | solution.py:86
  31.7 0.0 copy-start.8
  31.7 0.1 reshape.206
  31.9 0.0 copy-done
  31.9 1.2 convolution_convert_fusion.3
  33.1 0.0 all-reduce.3.cloned.1.call-update
  33.1 0.0 reduce-scatter.3.cloned.1.call-start
  33.1 0.0 copy-done.7
  33.2 0.1 copy.55
  33.3 0.1 eq.59
  33.4 0.2 fusion.23
  33.6 0.1 convert_element_type.118
  33.7 0.1 copy.56
  33.8 0.1 convert_reduce_fusion
  33.9 19.5 %all-reduce.3.cloned.1.call-done = bf16[64,2048]{1,0:T(8,128)(2,1)} async-done(((bf16[64,2048]{1,0:T(8,128)(2,1)}), bf16[64,2048]{1,0:T(8,128)(2,1)}) %all-reduce.3.cloned.1.call-update) | async-done | bytes 262160 | tf_op jit(solution)/shard_map/psum | solution.py:90
  53.4 0.0 copy-done.2
  53.4 1.1 fusion.42
  54.5 1.2 multiply_reduce_fusion
  55.7 0.0 copy-done.8
  55.7 1.1 multiply_convert_fusion
  56.8 0.7 convolution_convert_fusion.1
  57.5 0.0 copy-start.12
  57.6 53.7 %all_to_all.10 = bf16[16,32,2048]{2,1,0:T(8,128)(2,1)S(1)} all-to-all(bf16[16,32,2048]{2,1,0:T(8,128)(2,1)S(1)} %bitcast.62), channel_id=1, replica_groups=mesh['ep'=16,'tp'=2] {'ep'}, dimensions={0} | all-to-all | bytes 4194304 | tf_op jit(solution)/shard_map/all_to_all | solution.py:121
  111.3 1.3 copy-done.3
  112.6 0.0 copy-done.12
  112.6 0.7 fusion.31
  113.3 5.8 %convolution_convert_fusion = bf16[512,2048]{1,0:T(8,128)(2,1)} fusion(bf16[512,2048]{1,0:T(8,128)(2,1)} %bitcast.64, bf16[1,256,2048]{2,1,0:T(8,128)(2,1)} %param.33, bf16[1,2048,256]{2,1,0:T(8,128)(2,1)} %param.32, f32[512,256]{1,0:T(8,128)S(1)} %fusion.31), kind=kOutput, calls=%fused_computation.6 | convolution fusion | flops 1075576832 | bytes 6815744 | tf_op jit(solution)/shard_map/dot_general | solution.py:127
  119.1 0.0 reduce-scatter.3.cloned.1.call-update
  119.2 10.3 %reduce-scatter.3.cloned.1.call-done = bf16[512,1024]{1,0:T(8,128)(2,1)} async-done(((bf16[512,2048]{1,0:T(8,128)(2,1)}), bf16[512,1024]{1,0:T(8,128)(2,1)}) %reduce-scatter.3.cloned.1.call-update) | async-done | bytes 1048592 | tf_op jit(solution)/shard_map/reduce_scatter | solution.py:128
  129.5 6.4 %all-to-all-start.1 = ((bf16[16,32,1024]{2,1,0:T(8,128)(2,1)}), bf16[16,32,1024]{2,1,0:T(8,128)(2,1)}, u32[]{:S(2)}, u32[]{:S(2)}) async-start(bf16[16,32,1024]{2,1,0:T(8,128)(2,1)} %bitcast.65), calls=%async_computation.2 | async-start | bytes 2097152 | tf_op jit(solution)/shard_map/all_to_all | solution.py:132
  135.9 0.0 reduce-scatter.5.cloned.1.call-start
  135.9 0.0 copy-done.4
  135.9 0.8 convolution_convert_fusion.5
  136.8 0.0 copy-done.5
  136.8 0.8 convolution_convert_fusion.6
  137.6 1.5 fusion.67
  139.1 3.1 %convolution_convert_fusion.2 = bf16[64,2048]{1,0:T(8,128)(2,1)} fusion(bf16[256,2048]{1,0:T(8,128)(2,1)} %param.36, bf16[64,2048]{1,0:T(8,128)(2,1)S(1)} %multiply_convert_fusion, bf16[2048,256]{1,0:T(8,128)(2,1)} %param.35, f32[64,256]{1,0:T(8,128)S(1)} %fusion.67), kind=kOutput, calls=%fused_computation.8 | convolution fusion | flops 134447104 | bytes 2686976 | tf_op jit(solution)/shard_map/dot_general | solution.py:141
  142.2 0.0 reduce-scatter.5.cloned.1.call-update
  142.2 0.0 copy-done.6
  142.2 0.2 fusion.26
  142.5 17.8 %all-to-all-done.1 = bf16[16,32,1024]{2,1,0:T(8,128)(2,1)} async-done(((bf16[16,32,1024]{2,1,0:T(8,128)(2,1)}), bf16[16,32,1024]{2,1,0:T(8,128)(2,1)}, u32[]{:S(2)}, u32[]{:S(2)}) %all-to-all-start.1) | async-done | bytes 1048608 | tf_op jit(solution)/shard_map/all_to_all | solution.py:132
  160.3 1.7 fusion.17
  162.0 0.0 reduce-scatter.5.cloned.1.call-done
  162.0 1.1 fusion.64
  163.1 4.5 %all-reduce = (f32[64]{0:T(128)S(1)}, f32[64]{0:T(128)S(1)}) all-reduce(f32[64]{0:T(128)S(1)} %get-tuple-element.4, f32[64]{0:T(128)S(1)} %get-tuple-element.3), channel_id=1, replica_groups=mesh['ep'=16,'tp'=2] {'tp'}, use_global_device_ids=true, to_apply=%region_14.15 | all-reduce | flops 128 | bytes 1024 | tf_op jit(solution)/shard_map/psum | solution.py:147
  167.7 0.0 copy-done.9
  167.7 0.8 multiply_convert_fusion.1
  (15 shorter events, 0.1 us)
Async XLA Ops:
  7.2 24.7 %copy-start = (bf16[512,2048]{1,0:T(8,128)(2,1)S(1)}, bf16[512,2048]{1,0:T(8,128)(2,1)}, u32[]{:S(2)}) copy-start(bf16[512,2048]{1,0:T(8,128)(2,1)} %param.27) | copy-start | bytes 6291460
  7.2 2.5 %copy-start.10 = (s32[64]{0:T(128)S(1)}, s32[64]{0:T(128)}, u32[]{:S(2)}) copy-start(s32[64]{0:T(128)} %param.22) | copy-start | bytes 772
  7.2 46.2 %all-reduce.3.cloned.1.call-start = ((), (), s32[]{:S(2)}) async-start(), calls=%async_computation.4 | async-start | bytes 524288 | tf_op jit(solution)/shard_map/psum | solution.py:90
  9.8 4.6 %copy-start.11 = (f32[8]{0:T(128)S(1)}, f32[8]{0:T(128)}, u32[]{:S(2)}) copy-start(f32[8]{0:T(128)} %param.26) | copy-start | bytes 100
  14.4 3.0 %copy-start.1 = (f32[64,8,1024]{2,1,0:T(8,128)}, f32[64,8,1024]{2,1,0:T(8,128)S(1)}, u32[]{:S(2)}) copy-start(f32[64,8,1024]{2,1,0:T(8,128)S(1)} %fusion.2) | copy-start | bytes 6291460
  31.7 1.4 copy-start.7
  31.7 21.6 %copy-start.2 = (bf16[64,2048]{1,0:T(8,128)(2,1)S(1)}, bf16[64,2048]{1,0:T(8,128)(2,1)}, u32[]{:S(2)}) copy-start(bf16[64,2048]{1,0:T(8,128)(2,1)} %param.19) | copy-start | bytes 786436
  31.7 24.0 %copy-start.8 = (f32[2048]{0:T(1024)S(1)}, f32[2048]{0:T(1024)}, u32[]{:S(2)}) copy-start(f32[2048]{0:T(1024)} %param.28) | copy-start | bytes 24580
  33.1 96.4 %reduce-scatter.3.cloned.1.call-start = ((), (), s32[]{:S(2)}) async-start(), calls=%async_computation.5 | async-start | bytes 3145728 | tf_op jit(solution)/shard_map/reduce_scatter | solution.py:128
  57.5 55.0 %copy-start.12 = (bf16[1,2048,256]{2,1,0:T(8,128)(2,1)S(1)}, bf16[1,2048,256]{2,1,0:T(8,128)(2,1)}, u32[]{:S(2)}) copy-start(bf16[1,2048,256]{2,1,0:T(8,128)(2,1)} %param.31) | copy-start | bytes 3145732
  111.3 1.3 copy-start.3
  119.1 16.8 %copy-start.4 = (bf16[2048,64]{0,1:T(8,128)(2,1)S(1)}, bf16[2048,64]{0,1:T(8,128)(2,1)}, u32[]{:S(2)}) copy-start(bf16[2048,64]{0,1:T(8,128)(2,1)} %param.25) | copy-start | bytes 786436
  119.1 17.6 %copy-start.5 = (bf16[2048,64]{0,1:T(8,128)(2,1)S(1)}, bf16[2048,64]{0,1:T(8,128)(2,1)}, u32[]{:S(2)}) copy-start(bf16[2048,64]{0,1:T(8,128)(2,1)} %param.24) | copy-start | bytes 786436
  129.5 30.8 %all-to-all-start.1 = ((bf16[16,32,1024]{2,1,0:T(8,128)(2,1)}), bf16[16,32,1024]{2,1,0:T(8,128)(2,1)}, u32[]{:S(2)}, u32[]{:S(2)}) async-start(bf16[16,32,1024]{2,1,0:T(8,128)(2,1)} %bitcast.65), calls=%async_computation.2 | async-start | bytes 2097152 | tf_op jit(solution)/shard_map/all_to_all | solution.py:132
  135.9 26.1 %reduce-scatter.5.cloned.1.call-start = ((), (), s32[]{:S(2)}) async-start(), calls=%async_computation.6 | async-start | bytes 393216 | tf_op jit(solution)/shard_map/reduce_scatter | solution.py:142
  137.6 4.6 %copy-start.6 = (bf16[2048,16]{0,1:T(8,128)(2,1)S(1)}, bf16[2048,16]{0,1:T(8,128)(2,1)}, u32[]{:S(2)}) copy-start(bf16[2048,16]{0,1:T(8,128)(2,1)} %param.29) | copy-start | bytes 196612
  142.2 25.4 %copy-start.9 = (f32[1024]{0:T(1024)S(1)}, f32[1024]{0:T(1024)}, u32[]{:S(2)}) copy-start(f32[1024]{0:T(1024)} %param.37) | copy-start | bytes 12292
Sparse Core Ops, SparseCore 0:
  33.2 20.0 all-reduce.2
  119.3 10.1 reduce-scatter.2
  142.4 9.5 reduce-scatter.4
where the time goes:
time: 176 us; the launch traced here: 175 us
  blocking collectives  58.3 us (33%)
  waiting for transfers between devices  47.6 us (27%)
  matrix products  35 us (20%)
  between operations  14 us (8%)
  other arithmetic  8.58 us (5%)
  starting transfers between devices  6.54 us (4%)
  local copies, waits for them, and re-layouts  4.99 us (3%)
    all_to_all x1, blocking collectives, on_device(): lax.all_to_all(outgoing, 'ep', split_axis=0, concat_axis=0, tiled=True)  53.7 us
    psum x1, waiting for transfers between devices, on_device(): lax.psum(jnp.dot(attended, out_weight, preferred_element_type=jnp.float32...  19.5 us
    all_to_all x1, waiting for transfers between devices, on_device(): lax.all_to_all(back_rows, 'ep', split_axis=0, concat_axis=0, tiled=True)  17.8 us
    reduce_scatter x1, waiting for transfers between devices, on_device(): lax.psum_scatter(partial_value.astype(jnp.bfloat16), 'tp', scatter_dimens...  10.3 us
    dot_general x1, matrix products, on_device(): jnp.einsum('skgc,skdc->skgd', stick_weight, cache_values, preferred_eleme...  7 us
    all_to_all x1, starting transfers between devices, on_device(): lax.all_to_all(back_rows, 'ep', split_axis=0, concat_axis=0, tiled=True)  6.42 us
    dot_general x1, matrix products, on_device(): jnp.dot(inner, expert_down[0], preferred_element_type=jnp.float32)  5.83 us
    dot_general x1, matrix products, on_device(): jnp.einsum('skgd,skdc->skgc', query, cache_keys, preferred_element_type=j...  4.58 us
  transfers between devices with their start and end apart: 4, of which 3 were waited for; matrix products, arithmetic and copies ran while one was open for 5% of the time, Pallas kernels for 0%

commit v1 on v0

--- a/solution.py
+++ b/solution.py
@@ -7,6 +7,11 @@
 RESIDUAL_SCALE = 2.0**0.25
 ROUTE_SCALE = 2.5
 NORM_EPS = 1e-05
+
+
+def summed_here(x, mesh_axis):
+    parts = lax.all_gather(x, mesh_axis)
+    return jnp.sum(parts, axis=0)
 
 
 def layer_norm(values, gain_vec):
@@ -87,7 +92,7 @@
         "skgc,skdc->skgd", stick_weight, cache_values, preferred_element_type=jnp.float32
     )
     attended = attended.astype(jnp.bfloat16).reshape(seq_count, query_heads * head_size)
-    attention = lax.psum(
+    attention = summed_here(
         jnp.dot(attended, out_weight, preferred_element_type=jnp.float32).astype(jnp.bfloat16), "tp"
     ).astype(jnp.float32)
     hidden = layer_norm(

time: 176 us -> 156 us (0.89)
  waiting for transfers between devices: 47.6 us -> 28.1 us
  other arithmetic: 8.58 us -> 5.86 us
  blocking collectives: 58.3 us -> 61 us
    psum x1 -> x0, waiting for transfers between devices: 19.5 us -> none  [on_device(): lax.psum(jnp.dot(attended, out_weight, preferred_element_type=jnp.float32...]
    all_gather x0 -> x1, blocking collectives: none -> 2.48 us  [summed_here(): parts = lax.all_gather(x, mesh_axis)]
  transfers between devices with their start and end apart: 4 -> 3, of which waited for: 3 -> 2; matrix products, arithmetic and copies ran while one was open for 5% -> 5% of each run, Pallas kernels for 0% -> 0%
where the time goes in v1:
time: 156 us; the launch traced here: 155 us
  blocking collectives  61 us (39%)
  matrix products  34.3 us (22%)
  waiting for transfers between devices  28.1 us (18%)
  between operations  14.3 us (9%)
  starting transfers between devices  6.49 us (4%)
  other arithmetic  5.86 us (4%)
  local copies, waits for them, and re-layouts  5.01 us (3%)
    all_to_all x1, blocking collectives, on_device(): lax.all_to_all(outgoing, 'ep', split_axis=0, concat_axis=0, tiled=True)  54 us
    all_to_all x1, waiting for transfers between devices, on_device(): lax.all_to_all(back_rows, 'ep', split_axis=0, concat_axis=0, tiled=True)  17.7 us
    reduce_scatter x1, waiting for transfers between devices, on_device(): lax.psum_scatter(partial_value.astype(jnp.bfloat16), 'tp', scatter_dimens...  10.3 us
    dot_general x1, matrix products, on_device(): jnp.einsum('skgc,skdc->skgd', stick_weight, cache_values, preferred_eleme...  7 us
    all_to_all x1, starting transfers between devices, on_device(): lax.all_to_all(back_rows, 'ep', split_axis=0, concat_axis=0, tiled=True)  6.41 us
    dot_general x1, matrix products, on_device(): jnp.dot(inner, expert_down[0], preferred_element_type=jnp.float32)  5.83 us
    dot_general x1, matrix products, on_device(): jnp.einsum('skgd,skdc->skgc', query, cache_keys, preferred_element_type=j...  4.58 us
    psum x1, blocking collectives, on_device(): lax.psum((jnp.sum(mixed_rows, axis=1), jnp.sum(mixed_rows * mixed_rows, a...  4.52 us
  transfers between devices with their start and end apart: 3, of which 2 were waited for; matrix products, arithmetic and copies ran while one was open for 5% of the time, Pallas kernels for 0%

profile of v1, /device:TPU:9, one launch (start us, length us, event | category | flops | bytes accessed | tf_op | source)
XLA Modules:
  0.0 155.1 jit_solution(15640398480976909981)
XLA Ops:
  7.2 0.0 copy-start
  7.2 0.0 copy-start.10
  7.2 0.0 reduce-scatter.3.cloned.1.call-start
  7.2 2.3 %convolution_convert_fusion.4 = bf16[64,512]{1,0:T(8,128)(2,1)S(1)} fusion(bf16[64,2048]{1,0:T(8,128)(2,1)} %param.19, bf16[2048,512]{1,0:T(8,128)(2,1)} %param.23), kind=kOutput, calls=%fused_computation.27 | convolution fusion | flops 134250496 | bytes 2424832 | tf_op jit(solution)/shard_map/dot_general | solution.py:75
  9.5 0.1 reshape.201
  9.7 0.0 copy-done.10
  9.7 0.1 iota_compare_fusion.3
  9.8 0.0 copy-start.11
  9.8 4.6 %fusion.2 = f32[64,8,1024]{2,1,0:T(8,128)S(1)} fusion(bf16[64,8,64]{2,1,0:T(8,128)(2,1)S(1)} %reshape.201, bf16[64,1,64,1024]{3,2,1,0:T(8,128)(2,1)} %param.20), kind=kOutput, calls=%fused_computation.2 | convolution fusion | flops 67108864 | bytes 10551296 | tf_op jit(solution)/shard_map/skgd,skdc->skgc/dot_general | solution.py:81
  14.4 0.0 copy-done.11
  14.4 3.0 %fusion.65 = (f32[64,8,8]{1,2,0:T(8,128)S(1)}, f32[64,8,8,128]{3,1,2,0:T(8,128)}) fusion(f32[8]{0:T(128)S(1)} %copy-done.11, f32[64,8,1024]{2,1,0:T(8,128)S(1)} %fusion.2, pred[64,1024]{1,0:T(8,128)(4,1)S(1)} %iota_compare_fusion.3), kind=kLoop, calls=%fused_computation.95 | loop fusion | flops 5763072 | bytes 4276256 | tf_op jit(solution)/shard_map/reduce_sum | solution.py:39
  17.4 0.0 copy-done.1
  17.4 0.1 copy.53
  17.5 0.2 fusion.58
  17.7 0.1 copy.54
  17.8 4.2 %fusion.14 = f32[64,8,8,128]{3,2,1,0:T(8,128)} fusion(f32[64,8,8,128]{3,1,2,0:T(8,128)} %get-tuple-element.11, f32[64,8,8]{2,1,0:T(8,128)S(1)} %copy.54), kind=kOutput, calls=%fused_computation.21 | convolution fusion | flops 805847040 | bytes 4210688 | tf_op jit(solution)/shard_map/...bi,ic->...bc/dot_general | solution.py:36
  22.0 2.7 %reshape.204 = f32[64,8,1024]{2,1,0:T(8,128)} reshape(f32[64,8,8,128]{3,2,1,0:T(8,128)} %fusion.14) | data formatting | bytes 4194304 | tf_op jit(solution)/shard_map/reshape | solution.py:43
  24.7 7.0 %fusion.19 = bf16[64,8,64]{2,1,0:T(8,128)(2,1)S(1)} fusion(bf16[64,1,64,1024]{3,2,1,0:T(8,128)(2,1)} %param.21, f32[64,8,1024]{2,1,0:T(8,128)} %reshape.204, f32[64,8,1024]{2,1,0:T(8,128)} %copy-done.1, f32[8]{0:T(128)S(1)} %copy-done.11, pred[64,1024]{1,0:T(8,128)(4,1)S(1)} %iota_compare_fusion.3), kind=kOutput, calls=%fused_computation.26 | convolution fusion | flops 73957376 | bytes 12714016 | tf_op jit(solution)/shard_map/skgc,skdc->skgd/dot_general | solution.py:91
  31.7 0.1 reshape.206
  31.9 0.0 copy-done
  31.9 0.0 copy-start.7
  31.9 0.0 copy-start.8
  31.9 0.5 convolution_convert_fusion.3
  32.4 2.5 %all-gather = bf16[128,2048]{1,0:T(8,128)(2,1)S(1)} all-gather(bf16[64,2048]{1,0:T(8,128)(2,1)S(1)} %convolution_convert_fusion.3), channel_id=2, replica_groups=mesh['ep'=16,'tp'=2] {'tp'}, dimensions={0}, use_global_device_ids=true | all-gather | bytes 786432 | tf_op jit(solution)/shard_map/all_gather | solution.py:13
  34.9 0.1 reduce_sum.103
  35.0 0.0 copy-done.2
  35.0 0.2 fusion.42
  35.2 0.2 multiply_reduce_fusion
  35.4 0.0 copy-done.7
  35.5 0.1 copy.55
  35.5 0.1 eq.59
  35.7 0.2 fusion.23
  35.9 0.1 convert_element_type.120
  36.0 0.1 copy.56
  36.1 0.1 convert_reduce_fusion
  36.2 0.0 copy-done.8
  36.2 0.1 multiply_convert_fusion
  36.4 0.7 convolution_convert_fusion.1
  37.1 0.0 copy-start.12
  37.1 54.0 %all_to_all.10 = bf16[16,32,2048]{2,1,0:T(8,128)(2,1)S(1)} all-to-all(bf16[16,32,2048]{2,1,0:T(8,128)(2,1)S(1)} %bitcast.63), channel_id=1, replica_groups=mesh['ep'=16,'tp'=2] {'ep'}, dimensions={0} | all-to-all | bytes 4194304 | tf_op jit(solution)/shard_map/all_to_all | solution.py:126
  91.1 1.3 copy-done.3
  92.4 0.0 copy-done.12
  92.4 0.7 fusion.31
  93.1 5.8 %convolution_convert_fusion = bf16[512,2048]{1,0:T(8,128)(2,1)} fusion(bf16[512,2048]{1,0:T(8,128)(2,1)} %bitcast.65, bf16[1,256,2048]{2,1,0:T(8,128)(2,1)} %param.33, bf16[1,2048,256]{2,1,0:T(8,128)(2,1)} %param.32, f32[512,256]{1,0:T(8,128)S(1)} %fusion.31), kind=kOutput, calls=%fused_computation.6 | convolution fusion | flops 1075576832 | bytes 6815744 | tf_op jit(solution)/shard_map/dot_general | solution.py:132
  98.9 0.0 reduce-scatter.3.cloned.1.call-update
  98.9 10.3 %reduce-scatter.3.cloned.1.call-done = bf16[512,1024]{1,0:T(8,128)(2,1)} async-done(((bf16[512,2048]{1,0:T(8,128)(2,1)}), bf16[512,1024]{1,0:T(8,128)(2,1)}) %reduce-scatter.3.cloned.1.call-update) | async-done | bytes 1048592 | tf_op jit(solution)/shard_map/reduce_scatter | solution.py:133
  109.3 6.4 %all-to-all-start.1 = ((bf16[16,32,1024]{2,1,0:T(8,128)(2,1)}), bf16[16,32,1024]{2,1,0:T(8,128)(2,1)}, u32[]{:S(2)}, u32[]{:S(2)}) async-start(bf16[16,32,1024]{2,1,0:T(8,128)(2,1)} %bitcast.67), calls=%async_computation.2 | async-start | bytes 2097152 | tf_op jit(solution)/shard_map/all_to_all | solution.py:137
  115.7 0.0 copy-start.4
  115.7 0.0 reduce-scatter.5.cloned.1.call-start
  115.8 1.6 %fusion.67 = f32[64,256]{1,0:T(8,128)S(1)} fusion(bf16[64,2048]{1,0:T(8,128)(2,1)S(1)} %multiply_convert_fusion, bf16[2048,256]{1,0:T(8,128)(2,1)} %param.34), kind=kOutput, calls=%fused_computation.96 | convolution fusion | flops 67108864 | bytes 1376256 | tf_op jit(solution)/shard_map/dot_general | solution.py:143
  117.3 0.0 copy-start.5
  117.3 3.1 %convolution_convert_fusion.2 = bf16[64,2048]{1,0:T(8,128)(2,1)} fusion(bf16[256,2048]{1,0:T(8,128)(2,1)} %param.36, bf16[64,2048]{1,0:T(8,128)(2,1)S(1)} %multiply_convert_fusion, bf16[2048,256]{1,0:T(8,128)(2,1)} %param.35, f32[64,256]{1,0:T(8,128)S(1)} %fusion.67), kind=kOutput, calls=%fused_computation.8 | convolution fusion | flops 134447104 | bytes 2686976 | tf_op jit(solution)/shard_map/dot_general | solution.py:146
  120.4 0.0 reduce-scatter.5.cloned.1.call-update
  120.5 0.0 copy-done.6
  120.5 0.0 copy-start.9
  120.5 0.2 fusion.26
  120.7 0.8 convolution_convert_fusion.5
  121.5 0.8 convolution_convert_fusion.6
  122.4 17.7 %all-to-all-done.1 = bf16[16,32,1024]{2,1,0:T(8,128)(2,1)} async-done(((bf16[16,32,1024]{2,1,0:T(8,128)(2,1)}), bf16[16,32,1024]{2,1,0:T(8,128)(2,1)}, u32[]{:S(2)}, u32[]{:S(2)}) %all-to-all-start.1) | async-done | bytes 1048608 | tf_op jit(solution)/shard_map/all_to_all | solution.py:137
  140.1 1.7 %fusion.17 = f32[64,1024]{1,0:T(8,128)S(1)} fusion(bf16[512,1024,1]{1,0,2:T(8,128)(2,1)} %bitcast.15, f32[64,4]{0,1:T(4,128)S(1)} %multiply_divide_fusion, s32[64,4]{0,1:T(4,128)S(1)} %multiply_add_fusion.1), kind=kOutput, calls=%fused_computation.23 | convolution fusion | flops 269287424 | bytes 1312768 | tf_op jit(solution)/shard_map/dot_general | solution.py:138
  141.8 0.0 reduce-scatter.5.cloned.1.call-done
  141.8 1.1 fusion.64
  142.9 4.5 %all-reduce = (f32[64]{0:T(128)S(1)}, f32[64]{0:T(128)S(1)}) all-reduce(f32[64]{0:T(128)S(1)} %get-tuple-element.4, f32[64]{0:T(128)S(1)} %get-tuple-element.3), channel_id=1, replica_groups=mesh['ep'=16,'tp'=2] {'tp'}, use_global_device_ids=true, to_apply=%region_14.15 | all-reduce | flops 128 | bytes 1024 | tf_op jit(solution)/shard_map/psum | solution.py:152
  147.5 0.8 multiply_convert_fusion.1
  (14 shorter events, 0.1 us)
Async XLA Ops:
  7.2 24.7 %copy-start = (bf16[512,2048]{1,0:T(8,128)(2,1)S(1)}, bf16[512,2048]{1,0:T(8,128)(2,1)}, u32[]{:S(2)}) copy-start(bf16[512,2048]{1,0:T(8,128)(2,1)} %param.27) | copy-start | bytes 6291460
  7.2 2.5 %copy-start.10 = (s32[64]{0:T(128)S(1)}, s32[64]{0:T(128)}, u32[]{:S(2)}) copy-start(s32[64]{0:T(128)} %param.22) | copy-start | bytes 772
  7.2 102.1 %reduce-scatter.3.cloned.1.call-start = ((), (), s32[]{:S(2)}) async-start(), calls=%async_computation.4 | async-start | bytes 3145728 | tf_op jit(solution)/shard_map/reduce_scatter | solution.py:133
  9.8 4.6 %copy-start.11 = (f32[8]{0:T(128)S(1)}, f32[8]{0:T(128)}, u32[]{:S(2)}) copy-start(f32[8]{0:T(128)} %param.26) | copy-start | bytes 100
  14.4 3.0 %copy-start.1 = (f32[64,8,1024]{2,1,0:T(8,128)}, f32[64,8,1024]{2,1,0:T(8,128)S(1)}, u32[]{:S(2)}) copy-start(f32[64,8,1024]{2,1,0:T(8,128)S(1)} %fusion.2) | copy-start | bytes 6291460
  31.7 3.3 %copy-start.2 = (bf16[64,2048]{1,0:T(8,128)(2,1)S(1)}, bf16[64,2048]{1,0:T(8,128)(2,1)}, u32[]{:S(2)}) copy-start(bf16[64,2048]{1,0:T(8,128)(2,1)} %param.19) | copy-start | bytes 786436
  31.9 3.6 %copy-start.7 = (s32[64,4]{0,1:T(4,128)S(1)}, s32[64,4]{0,1:T(4,128)}, u32[]{:S(2)}) copy-start(s32[64,4]{0,1:T(4,128)} %param.30) | copy-start | bytes 3076
  31.9 4.3 %copy-start.8 = (f32[2048]{0:T(1024)S(1)}, f32[2048]{0:T(1024)}, u32[]{:S(2)}) copy-start(f32[2048]{0:T(1024)} %param.28) | copy-start | bytes 24580
  37.1 55.3 %copy-start.12 = (bf16[1,2048,256]{2,1,0:T(8,128)(2,1)S(1)}, bf16[1,2048,256]{2,1,0:T(8,128)(2,1)}, u32[]{:S(2)}) copy-start(bf16[1,2048,256]{2,1,0:T(8,128)(2,1)} %param.31) | copy-start | bytes 3145732
  91.1 1.3 copy-start.3
  109.3 30.8 %all-to-all-start.1 = ((bf16[16,32,1024]{2,1,0:T(8,128)(2,1)}), bf16[16,32,1024]{2,1,0:T(8,128)(2,1)}, u32[]{:S(2)}, u32[]{:S(2)}) async-start(bf16[16,32,1024]{2,1,0:T(8,128)(2,1)} %bitcast.67), calls=%async_computation.2 | async-start | bytes 2097152 | tf_op jit(solution)/shard_map/all_to_all | solution.py:137
  115.7 4.8 %copy-start.6 = (bf16[2048,16]{0,1:T(8,128)(2,1)S(1)}, bf16[2048,16]{0,1:T(8,128)(2,1)}, u32[]{:S(2)}) copy-start(bf16[2048,16]{0,1:T(8,128)(2,1)} %param.29) | copy-start | bytes 196612
  115.7 5.0 %copy-start.4 = (bf16[2048,64]{0,1:T(8,128)(2,1)S(1)}, bf16[2048,64]{0,1:T(8,128)(2,1)}, u32[]{:S(2)}) copy-start(bf16[2048,64]{0,1:T(8,128)(2,1)} %param.25) | copy-start | bytes 786436
  115.7 26.1 %reduce-scatter.5.cloned.1.call-start = ((), (), s32[]{:S(2)}) async-start(), calls=%async_computation.5 | async-start | bytes 393216 | tf_op jit(solution)/shard_map/reduce_scatter | solution.py:147
  117.3 4.2 %copy-start.5 = (bf16[2048,64]{0,1:T(8,128)(2,1)S(1)}, bf16[2048,64]{0,1:T(8,128)(2,1)}, u32[]{:S(2)}) copy-start(bf16[2048,64]{0,1:T(8,128)(2,1)} %param.24) | copy-start | bytes 786436
  120.5 27.0 %copy-start.9 = (f32[1024]{0:T(1024)S(1)}, f32[1024]{0:T(1024)}, u32[]{:S(2)}) copy-start(f32[1024]{0:T(1024)} %param.37) | copy-start | bytes 12292
Sparse Core Ops, SparseCore 0:
  99.1 10.1 reduce-scatter.2
  120.6 9.5 reduce-scatter.4
